TPU v7x, 32 devices: a whole 2x2x4 slice. The times are simulated.
32 devices in a mesh: grp: 2 (over y), fs: 8 (over z, core), tp: 2 (over x).
Axes of the slice: x: 2, y: 2, z: 4, core: 2. Of those that a mesh axis runs over, the one named last changes fastest.
Arguments:
- prompt: bfloat16 [6144, 2048], P(('grp', 'fs')), parts along dimension 0, may hold values from -6 to 6
- routes: int32 [6144, 4], P(('grp', 'fs')), parts along dimension 0, may hold values from 0 to 7, all different within a row; in each aligned block of 384 rows (0 to 383, 384 to 767, ...) at most 240 rows name the same one
- route_weight: float32 [6144, 4], P(('grp', 'fs')), parts along dimension 0, may hold values from 0.2 to 1
- norm_gain: float32 [2048], P('fs'), may hold values from 0.1 to 1.9
- gate_train: float32 [8, 2048, 1024], P(None, 'fs', 'tp'), may hold values from -0.4 to 0.4
- up_train: float32 [8, 2048, 1024], P(None, 'fs', 'tp'), may hold values from -0.4 to 0.4
- down_train: float32 [8, 1024, 2048], P(None, 'fs', 'tp'), may hold values from -0.07 to 0.07
Outputs:
- gate_serve: bfloat16 [16, 2048, 1024], P(('grp', 'fs'), None, 'tp'), parts along dimension 0
- up_serve: bfloat16 [16, 2048, 1024], P(('grp', 'fs'), None, 'tp'), parts along dimension 0
- down_serve: bfloat16 [16, 1024, 2048], P(('grp', 'fs'), 'tp'), parts along dimension 0
- mixed: bfloat16 [6144, 2048], P(('grp', 'fs'), 'tp'), parts along dimension 0
There are 2 independent parts, one for each index of `grp`. A program takes and returns all parts, laid end to end along the dimension named above; an argument that names none is the same for every part. Nothing has to cross between parts.
Inputs may be any that keep to these rules, and one draw needn't show every extreme that they name: `routes`: each row names 4 different experts. Among the rows of one index of fs no expert is named more than 240 times, a bound that some block reaches on some index.
All inputs are finite; a program needn't handle non-finite values.
Results may differ from a plain program's by a relative error of at most 0.012.
Values may be sent and summed in bfloat16 or wider, within the bound.
A program may use at most 128 MiB of HBM per device.

v0:
```python
import jax
import jax.numpy as jnp
from jax import lax
from jax.sharding import PartitionSpec as P

LIMIT = 7.0
ALPHA = 1.702
EPS = 1e-06


def shards(prompt, routes, route_weight, norm_gain, gate_train, up_train, down_train):
    tp = lax.axis_size("tp")
    experts = gate_train.shape[0]
    tok_rows, width = prompt.shape
    values = prompt.astype(jnp.float32)
    normed = (values * lax.rsqrt(jnp.mean(values * values, axis=-1, keepdims=True) + EPS)).astype(
        jnp.bfloat16
    )
    lanes = jnp.arange(experts, dtype=jnp.int32)
    scale = jnp.sum(
        jnp.where(routes[:, :, None] == lanes[None, None, :], route_weight[:, :, None], 0.0), axis=1
    )
    scale = lax.all_to_all(scale.T, "fs", split_axis=0, concat_axis=0, tiled=True)
    scale = scale.reshape(-1, 1)
    tokens = lax.all_gather(normed, "fs", axis=0, tiled=True)
    gain = norm_gain[None, :, None]
    gate_mine = lax.all_to_all(
        (gain * gate_train).astype(jnp.bfloat16), "fs", split_axis=0, concat_axis=0, tiled=True
    ).reshape(width, -1)
    up_mine = lax.all_to_all(
        (gain * up_train).astype(jnp.bfloat16), "fs", split_axis=0, concat_axis=0, tiled=True
    ).reshape(width, -1)
    down_rows = lax.all_to_all(
        down_train.astype(jnp.bfloat16), "fs", split_axis=0, concat_axis=0, tiled=True
    )
    down_rows = down_rows.reshape(-1, down_rows.shape[2])
    cols = down_rows.shape[1]
    own = gate_mine.shape[1]
    down_mine = lax.all_to_all(down_rows, "tp", split_axis=0, concat_axis=0, tiled=True)
    down_mine = down_mine.reshape(tp, own, cols).transpose(1, 0, 2).reshape(own, tp * cols)
    gate_pre = jnp.minimum(jnp.dot(tokens, gate_mine, preferred_element_type=jnp.float32), LIMIT)
    up_pre = jnp.clip(jnp.dot(tokens, up_mine, preferred_element_type=jnp.float32), -LIMIT, LIMIT)
    hidden = ((up_pre + 1.0) * gate_pre * jax.nn.sigmoid(ALPHA * gate_pre)).astype(jnp.bfloat16)
    pieces = lax.all_gather(hidden, "tp", axis=0, tiled=True)
    total = jnp.zeros((hidden.shape[0], cols), jnp.float32)
    for index in range(tp):
        total = total + jnp.dot(
            pieces[index * hidden.shape[0] : (index + 1) * hidden.shape[0]],
            down_rows[index * own : (index + 1) * own],
            preferred_element_type=jnp.float32,
        )
    weighted = (total * scale).astype(jnp.bfloat16)
    mixed = lax.psum_scatter(weighted, "fs", scatter_dimension=0, tiled=True)
    return (gate_mine[None], up_mine[None], down_mine[None], mixed)


def solution(mesh):
    return jax.shard_map(
        shards,
        mesh=mesh,
        in_specs=(
            P(("grp", "fs"), None),
            P(("grp", "fs"), None),
            P(("grp", "fs"), None),
            P("fs"),
            P(None, "fs", "tp"),
            P(None, "fs", "tp"),
            P(None, "fs", "tp"),
        ),
        out_specs=(
            P(("grp", "fs"), None, "tp"),
            P(("grp", "fs"), None, "tp"),
            P(("grp", "fs"), "tp", None),
            P(("grp", "fs"), "tp"),
        ),
        check_vma=False,
    )
```

profile of v0, /device:TPU:0, one launch (start us, length us, event | category | flops | bytes accessed | tf_op | source)
XLA Modules:
  0.0 429.3 jit_solution(14613814790445612276)
XLA Ops:
  7.2 0.0 copy-start.2
  7.2 0.0 all-gather.3.cloned.1.call-start
  7.2 1.8 fusion
  9.0 2.9 fusion.1
  11.9 0.0 all-gather.3.cloned.1.call-update
  11.9 0.0 copy-done.2
  11.9 6.1 %multiply_convert_fusion.2 = (bf16[8,256,512]{2,1,0:T(8,128)(2,1)}, bf16[8,256,512]{2,1,0:T(8,128)(2,1)S(1)}) fusion(f32[8,256,512]{2,1,0:T(8,128)} %param.12, f32[256]{0:T(256)S(1)} %copy-done.2, f32[8,256,512]{2,1,0:T(8,128)} %param.11), kind=kLoop, calls=%fused_computation.2 | loop fusion | flops 4194304 | bytes 12583936 | tf_op jit(solution)/shard_map/convert_element_type | solution.py:31
  18.1 111.5 %all_to_all.33 = bf16[8,256,512]{2,1,0:T(8,128)(2,1)S(1)} all-to-all(bf16[8,256,512]{2,1,0:T(8,128)(2,1)S(1)} %get-tuple-element.15), channel_id=1, replica_groups=mesh['grp'=2,'fs'=8,'tp'=2] {'fs'}, dimensions={0} | all-to-all | bytes 4194304 | tf_op jit(solution)/shard_map/all_to_all | solution.py:27
  129.6 4.3 %all-to-all-start.1 = ((bf16[8,256,512]{2,1,0:T(8,128)(2,1)}), bf16[8,256,512]{2,1,0:T(8,128)(2,1)}, u32[]{:S(2)}, u32[]{:S(2)}) async-start(bf16[8,256,512]{2,1,0:T(8,128)(2,1)} %get-tuple-element.14), calls=%async_computation.1 | async-start | bytes 4194304 | tf_op jit(solution)/shard_map/all_to_all | solution.py:30
  133.9 0.0 all-gather.5.cloned.1.call-start
  134.0 87.0 %all-gather.3.cloned.1.call-done = bf16[3072,2048]{1,0:T(8,128)(2,1)} async-done(((bf16[384,2048]{1,0:T(8,128)(2,1)}), bf16[3072,2048]{1,0:T(8,128)(2,1)}) %all-gather.3.cloned.1.call-update) | async-done | bytes 12582928 | tf_op jit(solution)/shard_map/all_gather | solution.py:25
  221.0 11.4 %fusion.6 = f32[3072,512]{1,0:T(8,128)} fusion(bf16[3072,2048]{1,0:T(8,128)(2,1)} %all-gather.3.cloned.1.call-done, bf16[2048,512]{1,0:T(8,128)(2,1)S(1)} %bitcast.20), kind=kOutput, calls=%fused_computation.15 | convolution fusion | flops 6442450944 | bytes 20971520 | tf_op jit(solution)/shard_map/dot_general | solution.py:41
  232.4 0.0 all-to-all-done.1
  232.4 15.8 %multiply_convert_fusion.1 = bf16[3072,512]{1,0:T(8,128)(2,1)} fusion(f32[3072,512]{1,0:T(8,128)} %fusion.6, bf16[3072,2048]{1,0:T(8,128)(2,1)} %all-gather.3.cloned.1.call-done, bf16[2048,512]{1,0:T(8,128)(2,1)} %bitcast.5), kind=kOutput, calls=%fused_computation.1 | convolution fusion | flops 6458179584 | bytes 24117248 | tf_op jit(solution)/shard_map/dot_general | solution.py:42
  248.1 0.0 all-gather.5.cloned.1.call-update
  248.1 0.0 copy-start
  248.1 0.0 copy-start.1
  248.2 3.8 convert_element_type.23
  252.0 4.4 %all-to-all-start.2 = ((bf16[8,128,1024]{2,1,0:T(8,128)(2,1)}), bf16[8,128,1024]{2,1,0:T(8,128)(2,1)}, u32[]{:S(2)}, u32[]{:S(2)}) async-start(bf16[8,128,1024]{2,1,0:T(8,128)(2,1)} %convert_element_type.23), calls=%async_computation.2 | async-start | bytes 4194304 | tf_op jit(solution)/shard_map/all_to_all | solution.py:33
  256.4 0.0 copy-done
  256.4 0.0 copy-done.1
  256.4 0.6 copy.24
  257.1 48.4 %all-to-all-done.2 = bf16[8,128,1024]{2,1,0:T(8,128)(2,1)} async-done(((bf16[8,128,1024]{2,1,0:T(8,128)(2,1)}), bf16[8,128,1024]{2,1,0:T(8,128)(2,1)}, u32[]{:S(2)}, u32[]{:S(2)}) %all-to-all-start.2) | async-done | bytes 2097184 | tf_op jit(solution)/shard_map/all_to_all | solution.py:33
  305.4 3.3 all-to-all-start.4
  308.8 0.2 reduce-scatter.2.cloned.1.call-start
  309.0 2.8 fusion.5
  311.8 15.0 %all-gather.5.cloned.1.call-done = bf16[6144,512]{1,0:T(8,128)(2,1)} async-done(((bf16[3072,512]{1,0:T(8,128)(2,1)}), bf16[6144,512]{1,0:T(8,128)(2,1)}) %all-gather.5.cloned.1.call-update) | async-done | bytes 6291472 | tf_op jit(solution)/shard_map/all_gather | solution.py:44
  326.8 10.1 %fusion.3 = f32[3072,1024]{1,0:T(8,128)} fusion(bf16[512,1024]{1,0:T(8,128)(2,1)} %bitcast.24, bf16[6144,512]{1,0:T(8,128)(2,1)} %all-gather.5.cloned.1.call-done), kind=kOutput, calls=%fused_computation.9 | convolution fusion | flops 3221225472 | bytes 16777216 | tf_op jit(solution)/shard_map/dot_general | solution.py:47
  336.9 0.0 all-to-all-done.4
  336.9 11.6 %multiply_convert_fusion = bf16[3072,1024]{1,0:T(8,128)(2,1)} fusion(f32[3072,1024]{1,0:T(8,128)} %fusion.3, f32[3072]{0:T(1024)S(1)} %bitcast.26, bf16[512,1024]{1,0:T(8,128)(2,1)S(1)} %bitcast.23, bf16[6144,512]{1,0:T(8,128)(2,1)} %all-gather.5.cloned.1.call-done), kind=kOutput, calls=%fused_computation | convolution fusion | flops 3230662656 | bytes 23080960 | tf_op jit(solution)/shard_map/dot_general | solution.py:47
  348.5 0.0 reduce-scatter.2.cloned.1.call-update
  348.6 4.8 %all-to-all-start.3 = ((bf16[2,512,1024]{2,1,0:T(8,128)(2,1)}), bf16[2,512,1024]{2,1,0:T(8,128)(2,1)}, u32[]{:S(2)}, u32[]{:S(2)}) async-start(bf16[2,512,1024]{2,1,0:T(8,128)(2,1)} %bitcast.2), calls=%async_computation.3 | async-start | bytes 4194304 | tf_op jit(solution)/shard_map/all_to_all | solution.py:39
  353.4 25.0 %all-to-all-done.3 = bf16[2,512,1024]{2,1,0:T(8,128)(2,1)} async-done(((bf16[2,512,1024]{2,1,0:T(8,128)(2,1)}), bf16[2,512,1024]{2,1,0:T(8,128)(2,1)}, u32[]{:S(2)}, u32[]{:S(2)}) %all-to-all-start.3) | async-done | bytes 2097184 | tf_op jit(solution)/shard_map/all_to_all | solution.py:39
  378.4 4.0 copy.23
  382.4 3.9 copy.25
  386.3 32.1 %reduce-scatter.2.cloned.1.call-done = bf16[384,1024]{1,0:T(8,128)(2,1)} async-done(((bf16[3072,1024]{1,0:T(8,128)(2,1)}), bf16[384,1024]{1,0:T(8,128)(2,1)}) %reduce-scatter.2.cloned.1.call-update) | async-done | bytes 786448 | tf_op jit(solution)/shard_map/reduce_scatter | solution.py:53
  418.4 1.3 copy.28
  419.8 3.0 copy.29
  (2 shorter events, 0.0 us)
Async XLA Ops:
  7.2 4.8 %copy-start.2 = (f32[256]{0:T(256)S(1)}, f32[256]{0:T(256)}, u32[]{:S(2)}) copy-start(f32[256]{0:T(256)} %param.10) | copy-start | bytes 3076
  7.2 213.8 %all-gather.3.cloned.1.call-start = ((), (), s32[]{:S(2)}) async-start(), calls=%async_computation.6 | async-start | bytes 14155776 | tf_op jit(solution)/shard_map/all_gather | solution.py:25
  129.6 102.8 %all-to-all-start.1 = ((bf16[8,256,512]{2,1,0:T(8,128)(2,1)}), bf16[8,256,512]{2,1,0:T(8,128)(2,1)}, u32[]{:S(2)}, u32[]{:S(2)}) async-start(bf16[8,256,512]{2,1,0:T(8,128)(2,1)} %get-tuple-element.14), calls=%async_computation.1 | async-start | bytes 4194304 | tf_op jit(solution)/shard_map/all_to_all | solution.py:30
  133.9 192.8 %all-gather.5.cloned.1.call-start = ((), (), s32[]{:S(2)}) async-start(), calls=%async_computation.7 | async-start | bytes 9437184 | tf_op jit(solution)/shard_map/all_gather | solution.py:44
  248.1 8.3 %copy-start = (f32[384,4]{0,1:T(4,128)S(1)}, f32[384,4]{0,1:T(4,128)}, u32[]{:S(2)}) copy-start(f32[384,4]{0,1:T(4,128)} %param.9) | copy-start | bytes 18436
  248.1 8.3 %copy-start.1 = (s32[384,4]{0,1:T(4,128)S(1)}, s32[384,4]{0,1:T(4,128)}, u32[]{:S(2)}) copy-start(s32[384,4]{0,1:T(4,128)} %param.8) | copy-start | bytes 18436
  252.0 53.4 %all-to-all-start.2 = ((bf16[8,128,1024]{2,1,0:T(8,128)(2,1)}), bf16[8,128,1024]{2,1,0:T(8,128)(2,1)}, u32[]{:S(2)}, u32[]{:S(2)}) async-start(bf16[8,128,1024]{2,1,0:T(8,128)(2,1)} %convert_element_type.23), calls=%async_computation.2 | async-start | bytes 4194304 | tf_op jit(solution)/shard_map/all_to_all | solution.py:33
  305.4 31.5 %all-to-all-start.4 = ((f32[8,1,384]{2,1,0:T(1,128)}), f32[8,1,384]{2,1,0:T(1,128)S(1)}, u32[]{:S(2)}, u32[]{:S(2)}) async-start(f32[8,1,384]{2,1,0:T(1,128)} %copy.24), calls=%async_computation.4 | async-start | bytes 24576 | tf_op jit(solution)/shard_map/all_to_all | solution.py:23
  308.8 109.7 %reduce-scatter.2.cloned.1.call-start = ((), (), s32[]{:S(2)}) async-start(), calls=%async_computation.8 | async-start | bytes 7077888 | tf_op jit(solution)/shard_map/reduce_scatter | solution.py:53
  348.6 29.9 %all-to-all-start.3 = ((bf16[2,512,1024]{2,1,0:T(8,128)(2,1)}), bf16[2,512,1024]{2,1,0:T(8,128)(2,1)}, u32[]{:S(2)}, u32[]{:S(2)}) async-start(bf16[2,512,1024]{2,1,0:T(8,128)(2,1)} %bitcast.2), calls=%async_computation.3 | async-start | bytes 4194304 | tf_op jit(solution)/shard_map/all_to_all | solution.py:39
Sparse Core Ops, SparseCore 0:
  12.0 208.8 all-gather.2
  248.3 78.4 all-gather.4
  348.7 69.7 reduce-scatter.1
where the time goes:
time: 430 us; the launch traced here: 429 us
  waiting for transfers between devices  208 us (48%)
  blocking collectives  112 us (26%)
  matrix products  48.9 us (11%)
  starting transfers between devices  17.2 us (4%)
  local copies, waits for them, and re-layouts  15.6 us (4%)
  other arithmetic  14.7 us (3%)
  between operations  13.8 us (3%)
    all_to_all x1, blocking collectives, shards(): lax.all_to_all((gain * gate_train).astype(jnp.bfloat16), 'fs', split_axis...  112 us
    all_gather x1, waiting for transfers between devices, shards(): tokens = lax.all_gather(normed, 'fs', axis=0, tiled=True)  87 us
    all_to_all x1, waiting for transfers between devices, shards(): lax.all_to_all(down_train.astype(jnp.bfloat16), 'fs', split_axis=0, conca...  48.4 us
    reduce_scatter x1, waiting for transfers between devices, shards(): mixed = lax.psum_scatter(weighted, 'fs', scatter_dimension=0, tiled=True)  32.1 us
    all_to_all x1, waiting for transfers between devices, shards(): lax.all_to_all(down_rows, 'tp', split_axis=0, concat_axis=0, tiled=True)  25 us
    dot_general x2, matrix products, shards(): jnp.dot(pieces[index * hidden.shape[0]:(index + 1) * hidden.shape[0]], do...  21.8 us
    dot_general x1, matrix products, shards(): jnp.dot(tokens, up_mine, preferred_element_type=jnp.float32)  15.8 us
    all_gather x1, waiting for transfers between devices, shards(): pieces = lax.all_gather(hidden, 'tp', axis=0, tiled=True)  15 us
  transfers between devices with their start and end apart: 7, of which 5 were waited for; matrix products, arithmetic and copies ran while one was open for 10% of the time, Pallas kernels for 0%

commit v1 on v0

--- a/solution.py
+++ b/solution.py
@@ -22,7 +22,9 @@
     )
     scale = lax.all_to_all(scale.T, "fs", split_axis=0, concat_axis=0, tiled=True)
     scale = scale.reshape(-1, 1)
-    tokens = lax.all_gather(normed, "fs", axis=0, tiled=True)
+    tokens = jnp.concatenate(
+        lax.all_to_all(jnp.stack([normed] * lax.axis_size("fs")), "fs", 0, 0), axis=0
+    )
     gain = norm_gain[None, :, None]
     gate_mine = lax.all_to_all(
         (gain * gate_train).astype(jnp.bfloat16), "fs", split_axis=0, concat_axis=0, tiled=True

time: 430 us -> 610 us (1.42)
  blocking collectives: 112 us -> 280 us
  local copies, waits for them, and re-layouts: 15.6 us -> 23.3 us
  starting transfers between devices: 17.2 us -> 23.5 us
    all_to_all x1, blocking collectives: 112 us -> 280 us  [shards(): lax.all_to_all(jnp.stack([normed] * lax.axis_size('fs')), 'fs', 0, 0)]
    all_gather x1 -> x0, waiting for transfers between devices: 87 us -> none  [shards(): tokens = lax.all_gather(normed, 'fs', axis=0, tiled=True)]
    all_to_all x0 -> x1, waiting for transfers between devices: none -> 44.4 us  [shards(): lax.all_to_all((gain * gate_train).astype(jnp.bfloat16), 'fs', split_axis...]
    all_to_all x1, waiting for transfers between devices: 0.01 us -> 37.6 us  [shards(): lax.all_to_all((gain * up_train).astype(jnp.bfloat16), 'fs', split_axis=0...]
    another operation x0 -> x1, local copies, waits for them, and re-layouts: none -> 7.64 us  [shards(): jnp.stack([normed] * lax.axis_size('fs'))]
    all_to_all x0 -> x1, starting transfers between devices: none -> 6.35 us  [shards(): lax.all_to_all((gain * gate_train).astype(jnp.bfloat16), 'fs', split_axis...]
  transfers between devices with their start and end apart: 7 -> 7, of which waited for: 5 -> 6; matrix products, arithmetic and copies ran while one was open for 10% -> 7% of each run, Pallas kernels for 0% -> 0%
where the time goes in v1:
time: 610 us; the launch traced here: 609 us
  blocking collectives  280 us (46%)
  waiting for transfers between devices  203 us (33%)
  matrix products  48.9 us (8%)
  starting transfers between devices  23.5 us (4%)
  local copies, waits for them, and re-layouts  23.3 us (4%)
  other arithmetic  15.4 us (3%)
  between operations  14.1 us (2%)
    all_to_all x1, blocking collectives, shards(): lax.all_to_all(jnp.stack([normed] * lax.axis_size('fs')), 'fs', 0, 0)  280 us
    all_to_all x1, waiting for transfers between devices, shards(): lax.all_to_all(down_train.astype(jnp.bfloat16), 'fs', split_axis=0, conca...  48.4 us
    all_to_all x1, waiting for transfers between devices, shards(): lax.all_to_all((gain * gate_train).astype(jnp.bfloat16), 'fs', split_axis...  44.4 us
    all_to_all x1, waiting for transfers between devices, shards(): lax.all_to_all((gain * up_train).astype(jnp.bfloat16), 'fs', split_axis=0...  37.6 us
    reduce_scatter x1, waiting for transfers between devices, shards(): mixed = lax.psum_scatter(weighted, 'fs', scatter_dimension=0, tiled=True)  32.1 us
    all_to_all x1, waiting for transfers between devices, shards(): lax.all_to_all(down_rows, 'tp', split_axis=0, concat_axis=0, tiled=True)  25 us
    dot_general x2, matrix products, shards(): jnp.dot(pieces[index * hidden.shape[0]:(index + 1) * hidden.shape[0]], do...  21.8 us
    all_gather x1, waiting for transfers between devices, shards(): pieces = lax.all_gather(hidden, 'tp', axis=0, tiled=True)  15.8 us
  transfers between devices with their start and end apart: 7, of which 6 were waited for; matrix products, arithmetic and copies ran while one was open for 7% of the time, Pallas kernels for 0%

profile of v1, /device:TPU:0, one launch (start us, length us, event | category | flops | bytes accessed | tf_op | source)
XLA Modules:
  0.0 608.9 jit_solution(6116758632087873872)
XLA Ops:
  7.2 6.8 %multiply_convert_fusion.2 = (bf16[8,256,512]{2,1,0:T(8,128)(2,1)}, bf16[8,256,512]{2,1,0:T(8,128)(2,1)}) fusion(f32[8,256,512]{2,1,0:T(8,128)} %param.12, f32[256]{0:T(256)} %param.10, f32[8,256,512]{2,1,0:T(8,128)} %param.11), kind=kLoop, calls=%fused_computation.2 | loop fusion | flops 4194304 | bytes 12583936 | tf_op jit(solution)/shard_map/convert_element_type | solution.py:33
  14.0 6.4 %all-to-all-start = ((bf16[8,256,512]{2,1,0:T(8,128)(2,1)}), bf16[8,256,512]{2,1,0:T(8,128)(2,1)S(1)}, u32[]{:S(2)}, u32[]{:S(2)}) async-start(bf16[8,256,512]{2,1,0:T(8,128)(2,1)} %get-tuple-element.15), calls=%async_computation | async-start | bytes 4194304 | tf_op jit(solution)/shard_map/all_to_all | solution.py:29
  20.3 1.8 fusion
  22.1 2.9 fusion.1
  25.0 44.4 %all-to-all-done = bf16[8,256,512]{2,1,0:T(8,128)(2,1)S(1)} async-done(((bf16[8,256,512]{2,1,0:T(8,128)(2,1)}), bf16[8,256,512]{2,1,0:T(8,128)(2,1)S(1)}, u32[]{:S(2)}, u32[]{:S(2)}) %all-to-all-start) | async-done | bytes 2097184 | tf_op jit(solution)/shard_map/all_to_all | solution.py:29
  69.4 7.6 %stack.2 = bf16[8,384,2048]{2,1,0:T(8,128)(2,1)} broadcast(bf16[384,2048]{1,0:T(8,128)(2,1)} %fusion.1), dimensions={1,2} | broadcast | bytes 14155776 | tf_op jit(solution)/shard_map/stack | solution.py:26
  77.0 280.5 %all_to_all.38 = bf16[8,384,2048]{2,1,0:T(8,128)(2,1)} all-to-all(bf16[8,384,2048]{2,1,0:T(8,128)(2,1)} %stack.2), channel_id=1, replica_groups=mesh['grp'=2,'fs'=8,'tp'=2] {'fs'}, dimensions={0} | all-to-all | bytes 25165824 | tf_op jit(solution)/shard_map/all_to_all | solution.py:26
  357.5 4.4 all-to-all-start.1
  361.9 0.0 all-gather.2.cloned.1.call-start
  361.9 11.4 %fusion.6 = f32[3072,512]{1,0:T(8,128)} fusion(bf16[3072,2048]{1,0:T(8,128)(2,1)} %bitcast.21, bf16[2048,512]{1,0:T(8,128)(2,1)S(1)} %bitcast.23), kind=kOutput, calls=%fused_computation.15 | convolution fusion | flops 6442450944 | bytes 20971520 | tf_op jit(solution)/shard_map/dot_general | solution.py:43
  373.3 37.6 %all-to-all-done.1 = bf16[8,256,512]{2,1,0:T(8,128)(2,1)} async-done(((bf16[8,256,512]{2,1,0:T(8,128)(2,1)}), bf16[8,256,512]{2,1,0:T(8,128)(2,1)}, u32[]{:S(2)}, u32[]{:S(2)}) %all-to-all-start.1) | async-done | bytes 2097184 | tf_op jit(solution)/shard_map/all_to_all | solution.py:32
  410.9 15.7 %multiply_convert_fusion.1 = bf16[3072,512]{1,0:T(8,128)(2,1)} fusion(f32[3072,512]{1,0:T(8,128)} %fusion.6, bf16[3072,2048]{1,0:T(8,128)(2,1)} %bitcast.22, bf16[2048,512]{1,0:T(8,128)(2,1)} %bitcast.6), kind=kOutput, calls=%fused_computation.1 | convolution fusion | flops 6458179584 | bytes 24117248 | tf_op jit(solution)/shard_map/dot_general | solution.py:44
  426.6 0.0 all-gather.2.cloned.1.call-update
  426.6 0.0 copy-start
  426.7 0.0 copy-start.1
  426.7 3.8 convert_element_type.23
  430.5 4.4 all-to-all-start.2
  434.9 0.0 copy-done
  434.9 0.0 copy-done.1
  434.9 0.6 copy.24
  435.6 48.4 %all-to-all-done.2 = bf16[8,128,1024]{2,1,0:T(8,128)(2,1)} async-done(((bf16[8,128,1024]{2,1,0:T(8,128)(2,1)}), bf16[8,128,1024]{2,1,0:T(8,128)(2,1)}, u32[]{:S(2)}, u32[]{:S(2)}) %all-to-all-start.2) | async-done | bytes 2097184 | tf_op jit(solution)/shard_map/all_to_all | solution.py:35
  483.9 3.3 all-to-all-start.5
  487.3 0.2 reduce-scatter.2.cloned.1.call-start
  487.5 2.8 fusion.5
  490.3 15.8 %all-gather.2.cloned.1.call-done = bf16[6144,512]{1,0:T(8,128)(2,1)} async-done(((bf16[3072,512]{1,0:T(8,128)(2,1)}), bf16[6144,512]{1,0:T(8,128)(2,1)}) %all-gather.2.cloned.1.call-update) | async-done | bytes 6291472 | tf_op jit(solution)/shard_map/all_gather | solution.py:46
  506.1 10.1 %fusion.3 = f32[3072,1024]{1,0:T(8,128)} fusion(bf16[512,1024]{1,0:T(8,128)(2,1)} %bitcast.27, bf16[6144,512]{1,0:T(8,128)(2,1)} %all-gather.2.cloned.1.call-done), kind=kOutput, calls=%fused_computation.9 | convolution fusion | flops 3221225472 | bytes 16777216 | tf_op jit(solution)/shard_map/dot_general | solution.py:49
  516.2 0.0 all-to-all-done.5
  516.2 11.6 %multiply_convert_fusion = bf16[3072,1024]{1,0:T(8,128)(2,1)} fusion(f32[3072,1024]{1,0:T(8,128)} %fusion.3, f32[3072]{0:T(1024)S(1)} %bitcast.29, bf16[512,1024]{1,0:T(8,128)(2,1)S(1)} %bitcast.26, bf16[6144,512]{1,0:T(8,128)(2,1)} %all-gather.2.cloned.1.call-done), kind=kOutput, calls=%fused_computation | convolution fusion | flops 3230662656 | bytes 23080960 | tf_op jit(solution)/shard_map/dot_general | solution.py:49
  527.8 0.0 reduce-scatter.2.cloned.1.call-update
  527.9 4.8 all-to-all-start.3
  532.7 25.0 %all-to-all-done.3 = bf16[2,512,1024]{2,1,0:T(8,128)(2,1)} async-done(((bf16[2,512,1024]{2,1,0:T(8,128)(2,1)}), bf16[2,512,1024]{2,1,0:T(8,128)(2,1)}, u32[]{:S(2)}, u32[]{:S(2)}) %all-to-all-start.3) | async-done | bytes 2097184 | tf_op jit(solution)/shard_map/all_to_all | solution.py:41
  557.7 4.0 copy.23
  561.7 3.9 copy.25
  565.7 32.1 %reduce-scatter.2.cloned.1.call-done = bf16[384,1024]{1,0:T(8,128)(2,1)} async-done(((bf16[3072,1024]{1,0:T(8,128)(2,1)}), bf16[384,1024]{1,0:T(8,128)(2,1)}) %reduce-scatter.2.cloned.1.call-update) | async-done | bytes 786448 | tf_op jit(solution)/shard_map/reduce_scatter | solution.py:55
  597.7 1.3 copy.28
  599.1 3.0 copy.29
  (2 shorter events, 0.0 us)
Async XLA Ops:
  14.0 55.4 %all-to-all-start = ((bf16[8,256,512]{2,1,0:T(8,128)(2,1)}), bf16[8,256,512]{2,1,0:T(8,128)(2,1)S(1)}, u32[]{:S(2)}, u32[]{:S(2)}) async-start(bf16[8,256,512]{2,1,0:T(8,128)(2,1)} %get-tuple-element.15), calls=%async_computation | async-start | bytes 4194304 | tf_op jit(solution)/shard_map/all_to_all | solution.py:29
  357.5 53.4 %all-to-all-start.1 = ((bf16[8,256,512]{2,1,0:T(8,128)(2,1)}), bf16[8,256,512]{2,1,0:T(8,128)(2,1)}, u32[]{:S(2)}, u32[]{:S(2)}) async-start(bf16[8,256,512]{2,1,0:T(8,128)(2,1)} %get-tuple-element.14), calls=%async_computation.1 | async-start | bytes 4194304 | tf_op jit(solution)/shard_map/all_to_all | solution.py:32
  361.9 144.2 %all-gather.2.cloned.1.call-start = ((), (), s32[]{:S(2)}) async-start(), calls=%async_computation.7 | async-start | bytes 9437184 | tf_op jit(solution)/shard_map/all_gather | solution.py:46
  426.6 8.3 %copy-start = (f32[384,4]{0,1:T(4,128)S(1)}, f32[384,4]{0,1:T(4,128)}, u32[]{:S(2)}) copy-start(f32[384,4]{0,1:T(4,128)} %param.9) | copy-start | bytes 18436
  426.7 8.3 %copy-start.1 = (s32[384,4]{0,1:T(4,128)S(1)}, s32[384,4]{0,1:T(4,128)}, u32[]{:S(2)}) copy-start(s32[384,4]{0,1:T(4,128)} %param.8) | copy-start | bytes 18436
  430.5 53.4 %all-to-all-start.2 = ((bf16[8,128,1024]{2,1,0:T(8,128)(2,1)}), bf16[8,128,1024]{2,1,0:T(8,128)(2,1)}, u32[]{:S(2)}, u32[]{:S(2)}) async-start(bf16[8,128,1024]{2,1,0:T(8,128)(2,1)} %convert_element_type.23), calls=%async_computation.2 | async-start | bytes 4194304 | tf_op jit(solution)/shard_map/all_to_all | solution.py:35
  483.9 32.3 %all-to-all-start.5 = ((f32[8,1,384]{2,1,0:T(1,128)}), f32[8,1,384]{2,1,0:T(1,128)S(1)}, u32[]{:S(2)}, u32[]{:S(2)}) async-start(f32[8,1,384]{2,1,0:T(1,128)} %copy.24), calls=%async_computation.5 | async-start | bytes 24576 | tf_op jit(solution)/shard_map/all_to_all | solution.py:23
  487.3 110.5 %reduce-scatter.2.cloned.1.call-start = ((), (), s32[]{:S(2)}) async-start(), calls=%async_computation.8 | async-start | bytes 7077888 | tf_op jit(solution)/shard_map/reduce_scatter | solution.py:55
  527.9 29.9 %all-to-all-start.3 = ((bf16[2,512,1024]{2,1,0:T(8,128)(2,1)}), bf16[2,512,1024]{2,1,0:T(8,128)(2,1)}, u32[]{:S(2)}, u32[]{:S(2)}) async-start(bf16[2,512,1024]{2,1,0:T(8,128)(2,1)} %bitcast.2), calls=%async_computation.3 | async-start | bytes 4194304 | tf_op jit(solution)/shard_map/all_to_all | solution.py:41
Sparse Core Ops, SparseCore 0:
  426.8 79.2 all-gather.1
  528.0 69.7 reduce-scatter.1
